TPU v7x, 32 devices: a whole 2x2x4 slice. The times are simulated.
32 devices in a mesh: grp: 2 (over y), fs: 4 (over z), tp: 4 (over x, core).
Axes of the slice: x: 2, y: 2, z: 4, core: 2. Of those that a mesh axis runs over, the one named last changes fastest.
Arguments:
- prompt: bfloat16 [2048, 2048], P(('grp', 'tp')), parts along dimension 0, may hold values from -6 to 6
- gain_first: float32 [2048], P('fs'), may hold values from 0.1 to 1.9
- gate_first: float32 [2048, 4096], P('fs', 'tp'), may hold values from -0.125 to 0.125
- up_first: float32 [2048, 4096], P('fs', 'tp'), may hold values from -0.125 to 0.125
- down_first: float32 [4096, 2048], P('fs', 'tp'), may hold values from -0.09375 to 0.09375
- gain_second: float32 [2048], P('fs'), may hold values from 0.1 to 1.9
- gate_second: float32 [2048, 4096], P('fs', 'tp'), may hold values from -0.125 to 0.125
- up_second: float32 [2048, 4096], P('fs', 'tp'), may hold values from -0.125 to 0.125
- down_second: float32 [4096, 2048], P('fs', 'tp'), may hold values from -0.09375 to 0.09375
Outputs:
- result: bfloat16 [2048, 2048], P(('grp', 'tp')), parts along dimension 0
- served_gate_first: bfloat16 [4096, 4096], P('grp', 'fs'), parts along dimension 0
- served_up_first: bfloat16 [4096, 4096], P('grp', 'fs'), parts along dimension 0
- served_down_first: bfloat16 [4096, 4096], P('fs', 'grp'), parts along dimension 1
- served_gate_second: bfloat16 [4096, 4096], P('grp', 'fs'), parts along dimension 0
- served_up_second: bfloat16 [4096, 4096], P('grp', 'fs'), parts along dimension 0
- served_down_second: bfloat16 [4096, 4096], P('fs', 'grp'), parts along dimension 1
There are 2 independent parts, one for each index of `grp`. A program takes and returns all parts, laid end to end along the dimension named above; an argument that names none is the same for every part. Nothing has to cross between parts.
All inputs are finite; a program needn't handle non-finite values.
Results may differ from a plain program's by a relative error of at most 0.0053.
Values may be sent and summed in bfloat16 or wider, within the bound.
A program may use at most 128 MiB of HBM per device.

v0:
```python
import jax
import jax.numpy as jnp
from jax import lax
from jax.sharding import PartitionSpec as P

EPS = 1e-06


def as_sent(array):
    return jax.tree.map(lambda a: a.astype(jnp.bfloat16) if a.dtype == jnp.float32 else a, array)


def fold(gain, weight):
    return (gain[:, None] * weight).astype(jnp.bfloat16)


def normed_of(stream):
    return (stream * lax.rsqrt(jnp.mean(stream * stream, axis=-1, keepdims=True) + EPS)).astype(
        jnp.bfloat16
    )


def hidden_of(normed, w_gate, w_up):
    gate = jnp.dot(normed, w_gate, preferred_element_type=jnp.float32)
    up_val = jnp.dot(normed, w_up, preferred_element_type=jnp.float32)
    return (jax.nn.silu(gate) * up_val).astype(jnp.bfloat16)


def on_device(
    prompt,
    gain_first,
    gate_first,
    up_first,
    down_first,
    gain_second,
    gate_second,
    up_second,
    down_second,
):
    folded = (
        fold(gain_first, gate_first),
        fold(gain_first, up_first),
        fold(gain_second, gate_second),
        fold(gain_second, up_second),
    )
    downs = (down_first.astype(jnp.bfloat16), down_second.astype(jnp.bfloat16))
    spread = (
        lax.all_to_all(folded[0], "tp", split_axis=0, concat_axis=1, tiled=True),
        lax.all_to_all(folded[1], "tp", split_axis=0, concat_axis=1, tiled=True),
        lax.all_to_all(folded[2], "tp", split_axis=0, concat_axis=1, tiled=True),
        lax.all_to_all(folded[3], "tp", split_axis=0, concat_axis=1, tiled=True),
    )
    moved = (
        lax.all_to_all(spread[0], "fs", split_axis=1, concat_axis=0, tiled=True),
        lax.all_to_all(spread[1], "fs", split_axis=1, concat_axis=0, tiled=True),
        lax.all_to_all(spread[2], "fs", split_axis=1, concat_axis=0, tiled=True),
        lax.all_to_all(spread[3], "fs", split_axis=1, concat_axis=0, tiled=True),
    )
    n_fs = lax.axis_size("fs")
    width = moved[0].shape[1]
    piece = moved[0].shape[0] // n_fs
    shaped = tuple((m.reshape(n_fs, piece, width) for m in moved))
    joined = jax.tree.map(
        lambda part, own: part.astype(own.dtype),
        lax.all_gather(as_sent(shaped), "tp", axis=1, tiled=True),
        shaped,
    )
    served = tuple((m.reshape(-1, width) for m in joined))
    served_downs = (
        lax.all_gather(downs[0], "tp", axis=1, tiled=True),
        lax.all_gather(downs[1], "tp", axis=1, tiled=True),
    )
    gates = (served[0], served[2])
    ups = (served[1], served[3])
    stream = prompt.astype(jnp.float32)
    for layer in range(2):
        hidden = hidden_of(normed_of(stream), gates[layer], ups[layer])
        partial_out = jnp.dot(hidden, served_downs[layer], preferred_element_type=jnp.float32)
        stream = stream + 0.5 * lax.psum(partial_out, "fs")
    result = stream.astype(jnp.bfloat16)
    return (result, served[0], served[1], served_downs[0], served[2], served[3], served_downs[1])


def solution(mesh):
    return jax.shard_map(
        on_device,
        mesh=mesh,
        in_specs=(
            P(("grp", "tp"), None),
            P("fs"),
            P("fs", "tp"),
            P("fs", "tp"),
            P("fs", "tp"),
            P("fs"),
            P("fs", "tp"),
            P("fs", "tp"),
            P("fs", "tp"),
        ),
        out_specs=(
            P(("grp", "tp"), None),
            P("grp", "fs"),
            P("grp", "fs"),
            P("fs", "grp"),
            P("grp", "fs"),
            P("grp", "fs"),
            P("fs", "grp"),
        ),
        check_vma=False,
    )
```

profile of v0, /device:TPU:0, one launch (start us, length us, event | category | flops | bytes accessed | tf_op | source)
XLA Modules:
  0.0 552.0 jit_solution(7371921522746309)
XLA Ops:
  7.2 0.0 all-gather.7.cloned.1.call-start
  7.2 2.5 multiply_convert_fusion.4
  9.7 18.5 %all_to_all.116 = bf16[4,128,1024]{2,1,0:T(8,128)(2,1)S(1)} all-to-all(bf16[4,128,1024]{2,1,0:T(8,128)(2,1)S(1)} %bitcast.43), channel_id=1, replica_groups=mesh['grp'=2,'fs'=4,'tp'=4] {'tp'}, dimensions={0} | all-to-all | bytes 2097152 | tf_op jit(solution)/shard_map/all_to_all | solution.py:48
  28.2 30.1 %all_to_all.117 = bf16[128,4,1024]{2,0,1:T(8,128)(2,1)} all-to-all(bf16[128,4,1024]{2,0,1:T(8,128)(2,1)S(1)} %bitcast.37), channel_id=1, replica_groups=mesh['grp'=2,'fs'=4,'tp'=4] {'fs'}, dimensions={1} | all-to-all | bytes 2097152 | tf_op jit(solution)/shard_map/all_to_all | solution.py:54
  58.4 0.0 all-gather.11.cloned.1.call-start
  58.4 2.7 convert_element_type.41
  61.1 0.0 all-gather.9.cloned.1.call-start
  61.2 28.0 %all_to_all.118 = bf16[4,128,1024]{2,1,0:T(8,128)(2,1)S(1)} all-to-all(bf16[4,128,1024]{2,1,0:T(8,128)(2,1)S(1)} %bitcast.42), channel_id=1, replica_groups=mesh['grp'=2,'fs'=4,'tp'=4] {'tp'}, dimensions={0} | all-to-all | bytes 2097152 | tf_op jit(solution)/shard_map/all_to_all | solution.py:49
  89.2 28.6 %all_to_all.119 = bf16[128,4,1024]{2,0,1:T(8,128)(2,1)} all-to-all(bf16[128,4,1024]{2,0,1:T(8,128)(2,1)S(1)} %bitcast.38), channel_id=1, replica_groups=mesh['grp'=2,'fs'=4,'tp'=4] {'fs'}, dimensions={1} | all-to-all | bytes 2097152 | tf_op jit(solution)/shard_map/all_to_all | solution.py:55
  117.9 3.5 multiply_convert_fusion.1
  121.4 3.6 all-to-all-start.4
  125.0 0.0 all-reduce.3.cloned.1.call-start
  125.1 0.3 fusion
  125.4 0.0 all-gather.7.cloned.1.call-done
  125.4 4.5 fusion.10
  129.9 14.3 %all-gather.11.cloned.1.call-done = bf16[1024,2048]{1,0:T(8,128)(2,1)} async-done(((bf16[1024,512]{1,0:T(8,128)(2,1)}), bf16[1024,2048]{1,0:T(8,128)(2,1)}) %all-gather.11.cloned.1.call-update) | async-done | bytes 4194320 | tf_op jit(solution)/shard_map/all_gather | solution.py:70
  144.1 38.1 %all-gather.9.cloned.1.call-done = bf16[4,512,1024]{2,1,0:T(8,128)(2,1)} async-done(((bf16[4,128,1024]{2,1,0:T(8,128)(2,1)}), bf16[4,512,1024]{2,1,0:T(8,128)(2,1)}) %all-gather.9.cloned.1.call-update) | async-done | bytes 4194320 | tf_op jit(solution)/shard_map/all_gather | solution.py:65
  182.2 7.6 %fusion.5 = f32[256,2048]{1,0:T(8,128)} fusion(bf16[1024,2048]{1,0:T(8,128)(2,1)} %all-gather.11.cloned.1.call-done, bf16[2048,1024]{1,0:T(8,128)(2,1)} %bitcast.26, f32[256,1024]{1,0:T(8,128)} %fusion.10, bf16[256,2048]{1,0:T(8,128)(2,1)S(1)} %copy-done.1, f32[256]{0:T(256)S(1)} %add_rsqrt_fusion.1), kind=kOutput, calls=%fused_computation.17 | convolution fusion | flops 2150629376 | bytes 12583936 | tf_op jit(solution)/shard_map/dot_general | solution.py:78
  189.9 0.0 all-gather.13.cloned.1.call-start
  189.9 57.0 %all_to_all.120 = bf16[128,4,1024]{2,0,1:T(8,128)(2,1)} all-to-all(bf16[128,4,1024]{2,0,1:T(8,128)(2,1)S(1)} %bitcast.34), channel_id=1, replica_groups=mesh['grp'=2,'fs'=4,'tp'=4] {'fs'}, dimensions={1} | all-to-all | bytes 2097152 | tf_op jit(solution)/shard_map/all_to_all | solution.py:56
  246.9 0.0 all-gather.17.cloned.1.call-start
  247.0 2.7 convert_element_type.46
  249.7 0.0 all-gather.15.cloned.1.call-start
  249.8 16.9 %all_to_all.121 = bf16[4,128,1024]{2,1,0:T(8,128)(2,1)S(1)} all-to-all(bf16[4,128,1024]{2,1,0:T(8,128)(2,1)S(1)} %bitcast.40), channel_id=1, replica_groups=mesh['grp'=2,'fs'=4,'tp'=4] {'tp'}, dimensions={0} | all-to-all | bytes 2097152 | tf_op jit(solution)/shard_map/all_to_all | solution.py:51
  266.6 52.7 %all_to_all.122 = bf16[128,4,1024]{2,0,1:T(8,128)(2,1)} all-to-all(bf16[128,4,1024]{2,0,1:T(8,128)(2,1)S(1)} %bitcast.39), channel_id=1, replica_groups=mesh['grp'=2,'fs'=4,'tp'=4] {'fs'}, dimensions={1} | all-to-all | bytes 2097152 | tf_op jit(solution)/shard_map/all_to_all | solution.py:57
  319.3 0.0 all-reduce.5.cloned.1.call-start
  319.4 0.5 all-reduce.3.cloned.1.call-done
  319.9 2.2 multiply_reduce_fusion
  322.0 0.0 copy-done
  322.1 1.3 multiply_convert_fusion.2
  323.4 31.3 %all-gather.13.cloned.1.call-done = bf16[4,512,1024]{2,1,0:T(8,128)(2,1)} async-done(((bf16[4,128,1024]{2,1,0:T(8,128)(2,1)}), bf16[4,512,1024]{2,1,0:T(8,128)(2,1)}) %all-gather.13.cloned.1.call-update) | async-done | bytes 4194320 | tf_op jit(solution)/shard_map/all_gather | solution.py:65
  354.7 4.7 fusion.14
  359.4 31.7 %all-gather.17.cloned.1.call-done = bf16[1024,2048]{1,0:T(8,128)(2,1)} async-done(((bf16[1024,512]{1,0:T(8,128)(2,1)}), bf16[1024,2048]{1,0:T(8,128)(2,1)}) %all-gather.17.cloned.1.call-update) | async-done | bytes 4194320 | tf_op jit(solution)/shard_map/all_gather | solution.py:71
  391.2 36.0 %all-gather.15.cloned.1.call-done = bf16[4,512,1024]{2,1,0:T(8,128)(2,1)} async-done(((bf16[4,128,1024]{2,1,0:T(8,128)(2,1)}), bf16[4,512,1024]{2,1,0:T(8,128)(2,1)}) %all-gather.15.cloned.1.call-update) | async-done | bytes 4194320 | tf_op jit(solution)/shard_map/all_gather | solution.py:65
  427.2 7.9 %fusion.4 = f32[256,2048]{1,0:T(8,128)} fusion(bf16[1024,2048]{1,0:T(8,128)(2,1)} %all-gather.17.cloned.1.call-done, bf16[256,2048]{1,0:T(8,128)(2,1)} %multiply_convert_fusion.2, bf16[2048,1024]{1,0:T(8,128)(2,1)} %bitcast.30, f32[256,1024]{1,0:T(8,128)} %fusion.14), kind=kOutput, calls=%fused_computation.16 | convolution fusion | flops 2149056512 | bytes 12582912 | tf_op jit(solution)/shard_map/dot_general | solution.py:78
  435.1 86.3 %all-reduce.5.cloned.1.call-done = f32[256,2048]{1,0:T(8,128)} async-done(((f32[256,2048]{1,0:T(8,128)}), f32[256,2048]{1,0:T(8,128)}) %all-reduce.5.cloned.1.call-update) | async-done | bytes 2097168 | tf_op jit(solution)/shard_map/psum | solution.py:79
  521.4 3.2 add_convert_fusion
  524.6 2.1 copy.24
  526.8 1.6 copy-done.4
  528.3 2.1 copy.25
  530.5 1.6 copy-done.3
  532.0 2.1 copy.26
  534.2 1.6 copy-done.5
  535.7 2.1 copy.27
  537.9 1.6 copy-done.7
  539.4 2.1 copy.28
  541.6 1.6 copy-done.6
  543.1 2.0 copy.29
  (23 shorter events, 0.2 us)
Async XLA Ops:
  7.2 118.2 %all-gather.7.cloned.1.call-start = ((), (), s32[]{:S(2)}) async-start(), calls=%async_computation.8 | async-start | bytes 5242880 | tf_op jit(solution)/shard_map/all_gather | solution.py:65
  58.4 85.8 %all-gather.11.cloned.1.call-start = ((), (), s32[]{:S(2)}) async-start(), calls=%async_computation.10 | async-start | bytes 5242880 | tf_op jit(solution)/shard_map/all_gather | solution.py:70
  61.1 121.1 %all-gather.9.cloned.1.call-start = ((), (), s32[]{:S(2)}) async-start(), calls=%async_computation.9 | async-start | bytes 5242880 | tf_op jit(solution)/shard_map/all_gather | solution.py:65
  89.2 28.6 %copy-start.8 = (f32[512]{0:T(512)S(1)}, f32[512]{0:T(512)}, u32[]{:S(2)}) copy-start(f32[512]{0:T(512)} %param.14) | copy-start | bytes 6148
  121.4 3.7 copy-start.1
  121.4 68.6 %all-to-all-start.4 = ((bf16[4,128,1024]{2,1,0:T(8,128)(2,1)}), bf16[4,128,1024]{2,1,0:T(8,128)(2,1)S(1)}, u32[]{:S(2)}, u32[]{:S(2)}) async-start(bf16[4,128,1024]{2,1,0:T(8,128)(2,1)} %bitcast.41), calls=%async_computation.4 | async-start | bytes 2097152 | tf_op jit(solution)/shard_map/all_to_all | solution.py:50
  125.0 194.8 %all-reduce.3.cloned.1.call-start = ((), (), s32[]{:S(2)}) async-start(), calls=%async_computation.11 | async-start | bytes 4194304 | tf_op jit(solution)/shard_map/psum | solution.py:79
  189.9 164.8 %all-gather.13.cloned.1.call-start = ((), (), s32[]{:S(2)}) async-start(), calls=%async_computation.12 | async-start | bytes 5242880 | tf_op jit(solution)/shard_map/all_gather | solution.py:65
  246.9 144.2 %all-gather.17.cloned.1.call-start = ((), (), s32[]{:S(2)}) async-start(), calls=%async_computation.14 | async-start | bytes 5242880 | tf_op jit(solution)/shard_map/all_gather | solution.py:71
  249.7 177.5 %all-gather.15.cloned.1.call-start = ((), (), s32[]{:S(2)}) async-start(), calls=%async_computation.13 | async-start | bytes 5242880 | tf_op jit(solution)/shard_map/all_gather | solution.py:65
  319.3 202.1 %all-reduce.5.cloned.1.call-start = ((), (), s32[]{:S(2)}) async-start(), calls=%async_computation.15 | async-start | bytes 4194304 | tf_op jit(solution)/shard_map/psum | solution.py:79
  319.9 2.2 copy-start
  521.4 3.2 copy-start.2
  524.6 3.7 copy-start.4
  528.3 3.7 copy-start.3
  532.0 3.7 copy-start.5
  535.7 3.7 copy-start.7
  539.4 3.7 copy-start.6
Sparse Core Ops, SparseCore 0:
  58.5 43.5 all-gather.6
  104.3 39.8 all-gather.10
  145.7 36.5 all-gather.8
  190.0 129.8 all-reduce.2
  321.3 33.3 all-gather.12
  356.7 34.4 all-gather.16
  392.7 34.4 all-gather.14
  435.2 86.1 all-reduce.4
where the time goes:
time: 553 us; the launch traced here: 552 us
  waiting for transfers between devices  238 us (43%)
  blocking collectives  232 us (42%)
  matrix products  24.7 us (4%)
  local copies, waits for them, and re-layouts  20.6 us (4%)
  other arithmetic  18.4 us (3%)
  between operations  14.2 us (3%)
    all_gather x4, waiting for transfers between devices, on_device(): lax.all_gather(as_sent(shaped), 'tp', axis=1, tiled=True)  106 us
    psum x2, waiting for transfers between devices, on_device(): stream = stream + 0.5 * lax.psum(partial_out, 'fs')  86.8 us
    all_to_all x1, blocking collectives, on_device(): lax.all_to_all(spread[2], 'fs', split_axis=1, concat_axis=0, tiled=True)  57 us
    all_to_all x1, blocking collectives, on_device(): lax.all_to_all(spread[3], 'fs', split_axis=1, concat_axis=0, tiled=True)  52.7 us
    all_gather x1, waiting for transfers between devices, on_device(): lax.all_gather(downs[1], 'tp', axis=1, tiled=True)  31.7 us
    all_to_all x1, blocking collectives, on_device(): lax.all_to_all(spread[0], 'fs', split_axis=1, concat_axis=0, tiled=True)  30.1 us
    all_to_all x1, blocking collectives, on_device(): lax.all_to_all(spread[1], 'fs', split_axis=1, concat_axis=0, tiled=True)  28.6 us
    all_to_all x1, blocking collectives, on_device(): lax.all_to_all(folded[1], 'tp', split_axis=0, concat_axis=1, tiled=True)  28 us
  transfers between devices with their start and end apart: 9, of which 7 were waited for; matrix products, arithmetic and copies ran while one was open for 5% of the time, Pallas kernels for 0%

commit v1 on v0

v1 whole, which is shorter than its diff:
```python
import functools

import jax
import jax.numpy as jnp
from jax import lax
from jax.experimental import pallas as pl
from jax.experimental.pallas import tpu as pltpu
from jax.sharding import PartitionSpec as P

EPS = 1e-06
MESH = pl.DeviceIdType.MESH


def fold(gain, weight):
    return (gain[:, None] * weight).astype(jnp.bfloat16)


def kernel(n_grp, n_fs, n_tp, *refs):
    prompt = refs[0]
    ins, in_down = refs[1:5], refs[5:7]
    out_result, outs, out_down = refs[7], refs[8:12], refs[12:14]
    served, served_down = refs[14:18], refs[18:20]
    stream, normed, hidden, part, landed, spread = refs[20:26]
    (z_send, z_recv, x_send, x_recv, y_send, y_recv, c_send, c_recv, own_sem,
     dx_send, dx_recv, dy_send, dy_recv, dc_send, dc_recv, down_own,
     rs_send, rs_recv, ag_send, ag_recv, out_sem) = refs[26:]

    g, f, t = lax.axis_index("grp"), lax.axis_index("fs"), lax.axis_index("tp")
    ratio = n_fs // n_tp
    chips = n_tp // 2
    home = f // ratio
    is_home = t == home
    is_lane = lax.rem(t, 2) == lax.rem(home, 2)
    partner = t + 1 - 2 * lax.rem(t, 2)

    def along_fs(o):
        return lax.rem(f + o, n_fs)

    def along_tp(dx):
        return lax.rem(t + 2 * dx, n_tp)

    def along_grp(dg):
        return lax.rem(g + dg, n_grp)

    barrier = pltpu.get_barrier_semaphore()
    peers = (
        [{"fs": along_fs(o)} for o in range(1, n_fs)]
        + [{"tp": along_tp(dx)} for dx in range(1, chips)]
        + [{"grp": along_grp(dg)} for dg in range(1, n_grp)]
        + [{"tp": partner}]
    )
    for peer in peers:
        pl.semaphore_signal(barrier, inc=1, device_id=peer, device_id_type=MESH)
    pl.semaphore_wait(barrier, len(peers))

    def remote(src, dst, send, recv, where):
        return pltpu.make_async_remote_copy(
            src_ref=src, dst_ref=dst, send_sem=send, recv_sem=recv,
            device_id=where, device_id_type=MESH,
        )

    def arrived(dst, sem):
        pltpu.make_async_copy(dst, dst, sem).wait()

    rows = ins[0].shape[0]
    share = rows // n_grp
    width = served[0].shape[1]
    d_rows = served_down[0].shape[0]
    d_share = d_rows // n_grp
    d_cols = in_down[0].shape[1]

    def piece(m, r, h):
        return served[m].at[pl.ds(pl.multiple_of(r * rows + h * share, share), share)]

    def z_copy(m, j):
        src = ins[m].at[pl.ds(pl.multiple_of(g * share, share), share), pl.ds(j * width, width)]
        return src, piece(m, f, g), t * ratio + j

    def z_start(m):
        for j in range(ratio):
            src, dst, to = z_copy(m, j)

            @pl.when(to != f)
            def _():
                remote(src, dst, z_send.at[m, j], z_recv.at[m, f], {"fs": to}).start()

            @pl.when(to == f)
            def _():
                pltpu.make_async_copy(src, dst, own_sem.at[m]).start()

    def x_copy(m, r, dx):
        ref = piece(m, r, g)
        return remote(ref, ref, x_send.at[m, r, dx - 1], x_recv.at[m, r], {"tp": along_tp(dx)})

    def y_copy(m, r, dg):
        ref = piece(m, r, g)
        return remote(ref, ref, y_send.at[m, r, dg - 1], y_recv.at[m, r, g], {"grp": along_grp(dg)})

    def c_copy(m, r, h):
        ref = piece(m, r, h)
        return remote(ref, ref, c_send.at[m, r, h], c_recv.at[m, r, h], {"tp": partner})

    def primary(m):
        @pl.when(is_lane)
        def _():
            @pl.loop(0, n_fs)
            def _(o):
                r = along_fs(o)

                @pl.when(is_home)
                def _():
                    @pl.when(o == 0)
                    def _():
                        arrived(piece(m, r, g), own_sem.at[m])

                    @pl.when(o != 0)
                    def _():
                        arrived(piece(m, r, g), z_recv.at[m, r])

                    for dx in range(1, chips):
                        x_copy(m, r, dx).start()

                @pl.when(jnp.logical_not(is_home))
                def _():
                    arrived(piece(m, r, g), x_recv.at[m, r])

                for dg in range(1, n_grp):
                    y_copy(m, r, dg).start()
                c_copy(m, r, g).start()

    def secondary(m):
        @pl.when(is_lane)
        def _():
            @pl.loop(0, n_fs)
            def _(o):
                r = along_fs(o)
                for dg in range(1, n_grp):
                    h = along_grp(dg)
                    arrived(piece(m, r, h), y_recv.at[m, r, h])
                    c_copy(m, r, h).start()

        @pl.when(jnp.logical_not(is_lane))
        def _():
            @pl.loop(0, n_fs)
            def _(r):
                for h in range(n_grp):
                    arrived(piece(m, r, h), c_recv.at[m, r, h])

        pltpu.make_async_copy(served[m], outs[m], out_sem.at[m]).start()

    def d_piece(k, s, h):
        return served_down[k].at[
            pl.ds(pl.multiple_of(h * d_share, d_share), d_share),
            pl.ds(pl.multiple_of(s * d_cols, d_cols), d_cols),
        ]

    def d_block(k, s):
        return served_down[k].at[:, pl.ds(pl.multiple_of(s * d_cols, d_cols), d_cols)]

    def dx_copy(k, dx):
        src = in_down[k].at[pl.ds(pl.multiple_of(g * d_share, d_share), d_share)]
        return remote(src, d_piece(k, t, g), dx_send.at[k, dx - 1], dx_recv.at[k, dx - 1], {"tp": along_tp(dx)})

    def dy_copy(k, dx, dg):
        ref = d_piece(k, lax.rem(t + n_tp - 2 * dx, n_tp), g)
        return remote(ref, ref, dy_send.at[k, dx - 1, dg - 1], dy_recv.at[k, dx - 1, dg - 1], {"grp": along_grp(dg)})

    def dc_own(k):
        return remote(in_down[k], d_block(k, t), dc_send.at[k, 0], dc_recv.at[k, 0], {"tp": partner})

    def dc_copy(k, dx):
        ref = d_block(k, lax.rem(t + n_tp - 2 * dx, n_tp))
        return remote(ref, ref, dc_send.at[k, dx], dc_recv.at[k, dx], {"tp": partner})

    def down_start(k):
        for dx in range(1, chips):
            dx_copy(k, dx).start()
        dc_own(k).start()
        pltpu.make_async_copy(in_down[k], d_block(k, t), down_own.at[k]).start()

    def down_primary(k):
        for dx in range(1, chips):
            source = lax.rem(t + n_tp - 2 * dx, n_tp)
            arrived(d_piece(k, source, g), dx_recv.at[k, dx - 1])
            for dg in range(1, n_grp):
                dy_copy(k, dx, dg).start()

    def down_secondary(k):
        for dx in range(1, chips):
            source = lax.rem(t + n_tp - 2 * dx, n_tp)
            for dg in range(1, n_grp):
                arrived(d_piece(k, source, lax.rem(g + n_grp - dg, n_grp)), dy_recv.at[k, dx - 1, dg - 1])
            dc_copy(k, dx).start()
        arrived(d_block(k, t), down_own.at[k])
        arrived(d_block(k, partner), dc_recv.at[k, 0])
        for dx in range(1, chips):
            arrived(d_block(k, lax.rem(partner + n_tp - 2 * dx, n_tp)), dc_recv.at[k, dx])
        pltpu.make_async_copy(served_down[k], out_down[k], out_sem.at[4 + k]).start()

    tokens, features = prompt.shape
    owned = tokens // n_fs
    slab = min(64, tokens)
    tile = min(256, width)
    wide = min(256, features)

    def rs_copy(k, o):
        to = along_fs(o)
        return remote(part.at[k, to], landed.at[k, f], rs_send.at[k, o - 1], rs_recv.at[k, f], {"fs": to})

    def ag_copy(k, o):
        return remote(spread.at[k, f], spread.at[k, f], ag_send.at[k, o - 1], ag_recv.at[k, f], {"fs": along_fs(o)})

    def multiply(k):
        w_gate, w_up, w_down = served[2 * k], served[2 * k + 1], served_down[k]

        @pl.loop(0, tokens // slab)
        def _(i):
            at = pl.ds(pl.multiple_of(i * slab, slab), slab)
            value = stream[at]
            scale = lax.rsqrt(jnp.mean(value * value, axis=-1, keepdims=True) + EPS)
            normed[at] = (value * scale).astype(jnp.bfloat16)

        @pl.loop(0, width // tile)
        def _(i):
            at = pl.ds(pl.multiple_of(i * tile, tile), tile)
            gate = jnp.dot(normed[...], w_gate[:, at], preferred_element_type=jnp.float32)
            up = jnp.dot(normed[...], w_up[:, at], preferred_element_type=jnp.float32)
            hidden[:, at] = (jax.nn.silu(gate) * up).astype(jnp.bfloat16)

    def project(k):
        w_down = served_down[k]

        @pl.loop(0, features // wide)
        def _(i):
            at = pl.ds(pl.multiple_of(i * wide, wide), wide)
            value = jnp.dot(hidden[...], w_down[:, at], preferred_element_type=jnp.float32)
            for to in range(n_fs):
                part[k, to, :, at] = value[to * owned : (to + 1) * owned].astype(jnp.bfloat16)

        for o in range(1, n_fs):
            rs_copy(k, o).start()

    def add_up(k, last):
        for o in range(1, n_fs):
            arrived(landed.at[k, along_fs(o)], rs_recv.at[k, along_fs(o)])
        mine = pl.ds(pl.multiple_of(f * owned, owned), owned)

        @pl.loop(0, features // wide)
        def _(i):
            at = pl.ds(pl.multiple_of(i * wide, wide), wide)
            total = part[k, f, :, at].astype(jnp.float32)
            for o in range(1, n_fs):
                total = total + landed[k, along_fs(o), :, at].astype(jnp.float32)
            total = 0.5 * total
            if last:
                total = stream[mine, at] + total
            spread[k, f, :, at] = total.astype(jnp.bfloat16)

        for o in range(1, n_fs):
            ag_copy(k, o).start()

    def collect(k):
        for o in range(1, n_fs):
            arrived(spread.at[k, along_fs(o)], ag_recv.at[k, along_fs(o)])

    for m in range(2):
        z_start(m)
    down_start(0)
    for m in range(2, 4):
        z_start(m)

    stream[...] = prompt[...].astype(jnp.float32)

    primary(0)
    primary(1)
    down_primary(0)
    secondary(0)
    secondary(1)
    down_start(1)
    multiply(0)
    down_secondary(0)
    project(0)
    primary(2)
    add_up(0, False)
    primary(3)
    down_primary(1)
    secondary(2)
    collect(0)
    for to in range(n_fs):
        at = pl.ds(to * owned, owned)
        stream[at] = stream[at] + spread[0, to].astype(jnp.float32)
    secondary(3)
    multiply(1)
    down_secondary(1)
    project(1)
    add_up(1, True)
    collect(1)
    result_copy = pltpu.make_async_copy(spread.at[1], out_result, out_sem.at[6])
    result_copy.start()

    for m in range(4):
        for j in range(ratio):
            src, dst, to = z_copy(m, j)

            @pl.when(to != f)
            def _():
                remote(src, dst, z_send.at[m, j], z_recv.at[m, f], {"fs": to}).wait_send()

        @pl.when(is_lane)
        def _():
            @pl.loop(0, n_fs)
            def _(r):
                @pl.when(is_home)
                def _():
                    for dx in range(1, chips):
                        x_copy(m, r, dx).wait_send()

                for dg in range(1, n_grp):
                    y_copy(m, r, dg).wait_send()
                for h in range(n_grp):
                    c_copy(m, r, h).wait_send()

        pltpu.make_async_copy(served[m], outs[m], out_sem.at[m]).wait()
    for k in range(2):
        dc_own(k).wait_send()
        for dx in range(1, chips):
            dx_copy(k, dx).wait_send()
            dc_copy(k, dx).wait_send()
            for dg in range(1, n_grp):
                dy_copy(k, dx, dg).wait_send()
        for o in range(1, n_fs):
            rs_copy(k, o).wait_send()
            ag_copy(k, o).wait_send()
        pltpu.make_async_copy(served_down[k], out_down[k], out_sem.at[4 + k]).wait()
    result_copy.wait()


def on_device(
    n_grp, n_fs, n_tp,
    prompt,
    gain_first,
    gate_first,
    up_first,
    down_first,
    gain_second,
    gate_second,
    up_second,
    down_second,
):
    own = (
        fold(gain_first, gate_first),
        fold(gain_first, up_first),
        fold(gain_second, gate_second),
        fold(gain_second, up_second),
        down_first.astype(jnp.bfloat16),
        down_second.astype(jnp.bfloat16),
    )
    tokens, features = prompt.shape
    width = gate_first.shape[1] * n_tp // n_fs
    d_rows = down_first.shape[0]
    owned = tokens // n_fs
    chips = n_tp // 2
    gate_shape, down_shape = (features, width), (d_rows, features)
    bf16 = functools.partial(jax.ShapeDtypeStruct, dtype=jnp.bfloat16)
    shapes = [(n_fs, owned, features)] + [gate_shape] * 4 + [down_shape] * 2
    other_x, other_g = max(chips - 1, 1), max(n_grp - 1, 1)
    sems = [
        (4, n_fs // n_tp), (4, n_fs), (4, n_fs, other_x), (4, n_fs), (4, n_fs, other_g),
        (4, n_fs, n_grp), (4, n_fs, n_grp), (4, n_fs, n_grp), (4,),
        (2, other_x), (2, other_x), (2, other_x, other_g), (2, other_x, other_g),
        (2, chips), (2, chips), (2,),
        (2, n_fs), (2, n_fs), (2, n_fs), (2, n_fs), (7,),
    ]
    result, g1, u1, g2, u2, d1, d2 = pl.pallas_call(
        functools.partial(kernel, n_grp, n_fs, n_tp),
        out_shape=[bf16(s) for s in shapes],
        in_specs=[pl.BlockSpec(memory_space=pltpu.VMEM)] + [pl.BlockSpec(memory_space=pl.ANY)] * 6,
        out_specs=[pl.BlockSpec(memory_space=pl.ANY)] * 7,
        scratch_shapes=[pltpu.VMEM(gate_shape, jnp.bfloat16)] * 4
        + [pltpu.VMEM(down_shape, jnp.bfloat16)] * 2
        + [
            pltpu.VMEM((tokens, features), jnp.float32),
            pltpu.VMEM((tokens, features), jnp.bfloat16),
            pltpu.VMEM((tokens, width), jnp.bfloat16),
            pltpu.VMEM((2, n_fs, owned, features), jnp.bfloat16),
            pltpu.VMEM((2, n_fs, owned, features), jnp.bfloat16),
            pltpu.VMEM((2, n_fs, owned, features), jnp.bfloat16),
        ]
        + [pltpu.SemaphoreType.DMA(s) for s in sems],
        compiler_params=pltpu.CompilerParams(
            collective_id=0, has_side_effects=True, vmem_limit_bytes=56 * 2**20
        ),
        name="serve",
    )(prompt, *own)
    return (result.reshape(tokens, features), g1, u1, d1, g2, u2, d2)


def solution(mesh):
    return jax.shard_map(
        functools.partial(on_device, mesh.shape["grp"], mesh.shape["fs"], mesh.shape["tp"]),
        mesh=mesh,
        in_specs=(
            P(("grp", "tp"), None),
            P("fs"),
            P("fs", "tp"),
            P("fs", "tp"),
            P("fs", "tp"),
            P("fs"),
            P("fs", "tp"),
            P("fs", "tp"),
            P("fs", "tp"),
        ),
        out_specs=(
            P(("grp", "tp"), None),
            P("grp", "fs"),
            P("grp", "fs"),
            P("fs", "grp"),
            P("grp", "fs"),
            P("grp", "fs"),
            P("fs", "grp"),
        ),
        check_vma=False,
    )
```

time: 553 us -> 270 us (0.49)
  waiting for transfers between devices: 238 us -> 0 us
  Pallas kernels: 0 us -> 235 us
  blocking collectives: 232 us -> 0 us
  matrix products: 24.7 us -> 0 us
  between operations: 14.2 us -> 0.67 us
  other arithmetic: 18.4 us -> 8.68 us
    pallas_call x0 -> x1, Pallas kernels: none -> 235 us  [on_device(): pl.pallas_call(functools.partial(kernel, n_grp, n_fs, n_tp), out_shape=[b...]
    all_to_all x7 -> x0, blocking collectives: 232 us -> none  [the longest x1 57 us: on_device(): lax.all_to_all(spread[2], 'fs', split_axis=1, concat_axis=0, tiled=True)]
    all_gather x6 -> x0, waiting for transfers between devices: 152 us -> none  [the longest x4 106 us: on_device(): lax.all_gather(as_sent(shaped), 'tp', axis=1, tiled=True)]
    psum x2 -> x0, waiting for transfers between devices: 86.8 us -> none  [on_device(): stream = stream + 0.5 * lax.psum(partial_out, 'fs')]
    dot_general x4 -> x0, matrix products: 24.7 us -> none  [the longest x2 15.5 us: on_device(): jnp.dot(hidden, served_downs[layer], preferred_element_type=jnp.float32)]
    convert_element_type x4 -> x2, other arithmetic: 9.9 us -> 3.95 us  [the longest x1 2.85 us: on_device(): down_first.astype(jnp.bfloat16)]
    unnamed x24 -> x23, local copies, waits for them, and re-layouts: 20.6 us -> 24.8 us
  transfers between devices with their start and end apart: 9 -> 0, of which waited for: 7 -> 0; matrix products, arithmetic and copies ran while one was open for 5% -> 0% of each run, Pallas kernels for 0% -> 0%
where the time goes in v1:
time: 270 us; the launch traced here: 269 us
  Pallas kernels  235 us (87%)
  local copies, waits for them, and re-layouts  24.8 us (9%)
  other arithmetic  8.68 us (3%)
    pallas_call x1, Pallas kernels, on_device(): pl.pallas_call(functools.partial(kernel, n_grp, n_fs, n_tp), out_shape=[b...  235 us
    unnamed x23, local copies, waits for them, and re-layouts  24.8 us

profile of v1, /device:TPU:0, one launch (start us, length us, event | category | flops | bytes accessed | tf_op | source)
XLA Modules:
  0.0 269.1 jit_solution(12687745122408053696)
XLA Ops:
  0.6 0.0 copy-start.5
  0.6 0.0 copy-start.7
  0.7 2.8 %convert_element_type.22.refs_5_ = bf16[1024,512]{1,0:T(8,128)(2,1)} convert(f32[1024,512]{1,0:T(8,128)} %param.13) | non-fusion elementwise | flops 524288 | bytes 3145728 | tf_op jit(solution)/shard_map/convert_element_type | solution.py:355
  3.5 0.0 copy-done.5
  3.5 0.0 copy-start.6
  3.5 1.1 convert_element_type.23.refs_6_
  4.6 0.0 copy-done.7
  4.6 0.9 copy-done.6
  5.5 4.7 %multiply_convert_fusion = (bf16[512,1024]{1,0:T(8,128)(2,1)}, bf16[512,1024]{1,0:T(8,128)(2,1)}, bf16[512,1024]{1,0:T(8,128)(2,1)}, bf16[512,1024]{1,0:T(8,128)(2,1)}) fusion(f32[512,1024]{1,0:T(8,128)S(1)} %copy-done.6, f32[512]{0:T(512)} %param.14, f32[512,1024]{1,0:T(8,128)S(1)} %copy-done.7, f32[512,1024]{1,0:T(8,128)} %param.11, f32[512]{0:T(512)} %param.10, ...), kind=kLoop, calls=%fused_computation | loop fusion | flops 4194304 | bytes 12587008 | tf_op jit(solution)/shard_map/convert_element_type | solution.py:15
  10.2 234.9 %serve.1 = (bf16[4,64,2048]{2,1,0:T(8,128)(2,1)}, bf16[2048,1024]{1,0:T(8,128)(2,1)}, bf16[2048,1024]{1,0:T(8,128)(2,1)}, bf16[2048,1024]{1,0:T(8,128)(2,1)}, bf...) custom-call(bf16[256,2048]{1,0:T(8,128)(2,1)} %refs_0_.1, ...), custom_call_target="tpu_custom_call" | custom-call | tf_op jit(solution)/shard_map/serve/pallas_call | solution.py:374
  245.1 2.3 copy.23
  247.5 0.0 copy-start.4
  247.5 4.8 %copy.24 = bf16[2048,1024]{1,0:T(8,128)(2,1)} copy(bf16[2048,1024]{1,0:T(8,128)(2,1)} %get-tuple-element.35) | data formatting | bytes 8388608
  252.3 0.0 copy-done.4
  252.3 0.0 copy-start.3
  252.3 2.1 copy.25
  254.4 1.6 copy-done.3
  256.0 0.0 copy-start.2
  256.0 2.1 copy.26
  258.1 1.6 copy-done.2
  259.7 0.0 copy-start.1
  259.7 2.1 copy.27
  261.8 1.6 copy-done.1
  263.4 0.0 copy-start
  263.4 2.1 copy.28
  265.5 1.6 copy-done
  267.1 2.0 copy.29
Async XLA Ops:
  0.6 2.9 %copy-start.5 = (f32[1024,512]{1,0:T(8,128)S(1)}, f32[1024,512]{1,0:T(8,128)}, u32[]{:S(2)}) copy-start(f32[1024,512]{1,0:T(8,128)} %param.17) | copy-start | bytes 6291460
  0.6 4.0 %copy-start.7 = (f32[512,1024]{1,0:T(8,128)S(1)}, f32[512,1024]{1,0:T(8,128)}, u32[]{:S(2)}) copy-start(f32[512,1024]{1,0:T(8,128)} %param.15) | copy-start | bytes 6291460
  3.5 2.0 copy-start.6
  247.5 4.8 %copy-start.4 = (bf16[2048,1024]{1,0:T(8,128)(2,1)S(1)}, bf16[2048,1024]{1,0:T(8,128)(2,1)}, u32[]{:S(2)}) copy-start(bf16[2048,1024]{1,0:T(8,128)(2,1)} %get-tuple-element.36) | copy-start | bytes 12582916
  252.3 3.7 %copy-start.3 = (bf16[1024,2048]{1,0:T(8,128)(2,1)S(1)}, bf16[1024,2048]{1,0:T(8,128)(2,1)}, u32[]{:S(2)}) copy-start(bf16[1024,2048]{1,0:T(8,128)(2,1)} %get-tuple-element.37) | copy-start | bytes 12582916
  256.0 3.7 %copy-start.2 = (bf16[2048,1024]{1,0:T(8,128)(2,1)S(1)}, bf16[2048,1024]{1,0:T(8,128)(2,1)}, u32[]{:S(2)}) copy-start(bf16[2048,1024]{1,0:T(8,128)(2,1)} %get-tuple-element.38) | copy-start | bytes 12582916
  259.7 3.7 %copy-start.1 = (bf16[2048,1024]{1,0:T(8,128)(2,1)S(1)}, bf16[2048,1024]{1,0:T(8,128)(2,1)}, u32[]{:S(2)}) copy-start(bf16[2048,1024]{1,0:T(8,128)(2,1)} %get-tuple-element.39) | copy-start | bytes 12582916
  263.4 3.7 %copy-start = (bf16[1024,2048]{1,0:T(8,128)(2,1)S(1)}, bf16[1024,2048]{1,0:T(8,128)(2,1)}, u32[]{:S(2)}) copy-start(bf16[1024,2048]{1,0:T(8,128)(2,1)} %get-tuple-element.40) | copy-start | bytes 12582916

commit v2 on v1

--- a/solution.py
+++ b/solution.py
@@ -15,21 +15,22 @@
     return (gain[:, None] * weight).astype(jnp.bfloat16)
 
 
-def kernel(n_grp, n_fs, n_tp, *refs):
+def kernel(n_grp, n_fs, n_tp, n_sub, *refs):
     prompt = refs[0]
     ins, in_down = refs[1:5], refs[5:7]
     out_result, outs, out_down = refs[7], refs[8:12], refs[12:14]
     served, served_down = refs[14:18], refs[18:20]
-    stream, normed, hidden, part, landed, spread = refs[20:26]
-    (z_send, z_recv, x_send, x_recv, y_send, y_recv, c_send, c_recv, own_sem,
+    stream, normed, hidden, part, landed, spread, stage = refs[20:27]
+    (p_send, p_recv, r_send, z_send, z_recv, x_send, x_recv, y_send, y_recv, c_send, c_recv, own_sem,
      dx_send, dx_recv, dy_send, dy_recv, dc_send, dc_recv, down_own,
-     rs_send, rs_recv, ag_send, ag_recv, out_sem) = refs[26:]
+     rs_send, rs_recv, ag_send, ag_recv, out_sem) = refs[27:]
 
     g, f, t = lax.axis_index("grp"), lax.axis_index("fs"), lax.axis_index("tp")
     ratio = n_fs // n_tp
     chips = n_tp // 2
     home = f // ratio
-    is_home = t == home
+    mine_sub = lax.rem(t + n_tp - home, n_tp) // 2
+    carries = mine_sub < n_sub
     is_lane = lax.rem(t, 2) == lax.rem(home, 2)
     partner = t + 1 - 2 * lax.rem(t, 2)
 
@@ -64,41 +65,60 @@
 
     rows = ins[0].shape[0]
     share = rows // n_grp
+    sub = share // n_sub
     width = served[0].shape[1]
     d_rows = served_down[0].shape[0]
     d_share = d_rows // n_grp
     d_cols = in_down[0].shape[1]
 
-    def piece(m, r, h):
-        return served[m].at[pl.ds(pl.multiple_of(r * rows + h * share, share), share)]
-
-    def z_copy(m, j):
-        src = ins[m].at[pl.ds(pl.multiple_of(g * share, share), share), pl.ds(j * width, width)]
-        return src, piece(m, f, g), t * ratio + j
-
-    def z_start(m):
+    def piece(m, r, h, s):
+        return served[m].at[pl.ds(pl.multiple_of(r * rows + h * share + s * sub, sub), sub)]
+
+    def p_copy(m, s):
+        src = ins[m].at[pl.ds(pl.multiple_of(g * share + s * sub, sub), sub)]
+        return remote(src, stage.at[m, s - 1], p_send.at[m, s - 1], p_recv.at[m, s - 1], {"tp": along_tp(s)})
+
+    def z_copy(m, s, j):
+        columns = pl.ds(j * width, width)
+        if s == 0:
+            src = ins[m].at[pl.ds(pl.multiple_of(g * share, share), sub), columns]
+            return src, piece(m, f, g, s), t * ratio + j
+        source = lax.rem(t + n_tp - 2 * s, n_tp)
+        return stage.at[m, s - 1, :, columns], piece(m, f, g, s), source * ratio + j
+
+    def z_remote(m, s, j):
+        src, dst, to = z_copy(m, s, j)
+        send = z_send.at[m, j] if s == 0 else r_send.at[m, s - 1, j]
+        return remote(src, dst, send, z_recv.at[m, f], {"fs": to})
+
+    def z_start(m, s):
         for j in range(ratio):
-            src, dst, to = z_copy(m, j)
+            src, dst, to = z_copy(m, s, j)
 
             @pl.when(to != f)
             def _():
-                remote(src, dst, z_send.at[m, j], z_recv.at[m, f], {"fs": to}).start()
+                z_remote(m, s, j).start()
 
             @pl.when(to == f)
             def _():
                 pltpu.make_async_copy(src, dst, own_sem.at[m]).start()
 
+    def relay(m):
+        for s in range(1, n_sub):
+            arrived(stage.at[m, s - 1], p_recv.at[m, s - 1])
+            z_start(m, s)
+
     def x_copy(m, r, dx):
-        ref = piece(m, r, g)
-        return remote(ref, ref, x_send.at[m, r, dx - 1], x_recv.at[m, r], {"tp": along_tp(dx)})
-
-    def y_copy(m, r, dg):
-        ref = piece(m, r, g)
-        return remote(ref, ref, y_send.at[m, r, dg - 1], y_recv.at[m, r, g], {"grp": along_grp(dg)})
-
-    def c_copy(m, r, h):
-        ref = piece(m, r, h)
-        return remote(ref, ref, c_send.at[m, r, h], c_recv.at[m, r, h], {"tp": partner})
+        ref = piece(m, r, g, mine_sub)
+        return remote(ref, ref, x_send.at[m, r, dx - 1], x_recv.at[m, r, mine_sub], {"tp": along_tp(dx)})
+
+    def y_copy(m, r, dg, s):
+        ref = piece(m, r, g, s)
+        return remote(ref, ref, y_send.at[m, r, dg - 1, s], y_recv.at[m, r, g, s], {"grp": along_grp(dg)})
+
+    def c_copy(m, r, h, s):
+        ref = piece(m, r, h, s)
+        return remote(ref, ref, c_send.at[m, r, h, s], c_recv.at[m, r, h, s], {"tp": partner})
 
     def primary(m):
         @pl.when(is_lane)
@@ -107,26 +127,35 @@
             def _(o):
                 r = along_fs(o)
 
-                @pl.when(is_home)
+                @pl.when(carries)
                 def _():
                     @pl.when(o == 0)
                     def _():
-                        arrived(piece(m, r, g), own_sem.at[m])
+                        arrived(piece(m, r, g, mine_sub), own_sem.at[m])
 
                     @pl.when(o != 0)
                     def _():
-                        arrived(piece(m, r, g), z_recv.at[m, r])
+                        arrived(piece(m, r, g, mine_sub), z_recv.at[m, r])
 
                     for dx in range(1, chips):
                         x_copy(m, r, dx).start()
-
-                @pl.when(jnp.logical_not(is_home))
-                def _():
-                    arrived(piece(m, r, g), x_recv.at[m, r])
-
-                for dg in range(1, n_grp):
-                    y_copy(m, r, dg).start()
-                c_copy(m, r, g).start()
+                    for dg in range(1, n_grp):
+                        y_copy(m, r, dg, mine_sub).start()
+                    c_copy(m, r, g, mine_sub).start()
+
+    def crossed(m):
+        @pl.when(is_lane)
+        def _():
+            @pl.loop(0, n_fs)
+            def _(o):
+                r = along_fs(o)
+                for s in range(n_sub):
+                    @pl.when(mine_sub != s)
+                    def _():
+                        arrived(piece(m, r, g, s), x_recv.at[m, r, s])
+                        for dg in range(1, n_grp):
+                            y_copy(m, r, dg, s).start()
+                        c_copy(m, r, g, s).start()
 
     def secondary(m):
         @pl.when(is_lane)
@@ -136,15 +165,17 @@
                 r = along_fs(o)
                 for dg in range(1, n_grp):
                     h = along_grp(dg)
-                    arrived(piece(m, r, h), y_recv.at[m, r, h])
-                    c_copy(m, r, h).start()
+                    for s in range(n_sub):
+                        arrived(piece(m, r, h, s), y_recv.at[m, r, h, s])
+                        c_copy(m, r, h, s).start()
 
         @pl.when(jnp.logical_not(is_lane))
         def _():
             @pl.loop(0, n_fs)
             def _(r):
                 for h in range(n_grp):
-                    arrived(piece(m, r, h), c_recv.at[m, r, h])
+                    for s in range(n_sub):
+                        arrived(piece(m, r, h, s), c_recv.at[m, r, h, s])
 
         pltpu.make_async_copy(served[m], outs[m], out_sem.at[m]).start()
 
@@ -263,33 +294,41 @@
         for o in range(1, n_fs):
             arrived(spread.at[k, along_fs(o)], ag_recv.at[k, along_fs(o)])
 
-    for m in range(2):
-        z_start(m)
-    down_start(0)
-    for m in range(2, 4):
-        z_start(m)
+    for m in range(4):
+        for s in range(1, n_sub):
+            p_copy(m, s).start()
+        z_start(m, 0)
+        if m % 2 == 1:
+            down_start(m // 2)
 
     stream[...] = prompt[...].astype(jnp.float32)
 
+    relay(0)
+    relay(1)
     primary(0)
+    relay(2)
     primary(1)
+    relay(3)
+    crossed(0)
+    primary(2)
+    crossed(1)
     down_primary(0)
+    primary(3)
     secondary(0)
     secondary(1)
-    down_start(1)
     multiply(0)
+    crossed(2)
     down_secondary(0)
     project(0)
-    primary(2)
-    add_up(0, False)
-    primary(3)
+    crossed(3)
     down_primary(1)
     secondary(2)
+    add_up(0, False)
+    secondary(3)
     collect(0)
     for to in range(n_fs):
         at = pl.ds(to * owned, owned)
         stream[at] = stream[at] + spread[0, to].astype(jnp.float32)
-    secondary(3)
     multiply(1)
     down_secondary(1)
     project(1)
@@ -299,26 +338,28 @@
     result_copy.start()
 
     for m in range(4):
-        for j in range(ratio):
-            src, dst, to = z_copy(m, j)
-
-            @pl.when(to != f)
-            def _():
-                remote(src, dst, z_send.at[m, j], z_recv.at[m, f], {"fs": to}).wait_send()
+        for s in range(n_sub):
+            if s > 0:
+                p_copy(m, s).wait_send()
+            for j in range(ratio):
+                @pl.when(z_copy(m, s, j)[2] != f)
+                def _():
+                    z_remote(m, s, j).wait_send()
 
         @pl.when(is_lane)
         def _():
             @pl.loop(0, n_fs)
             def _(r):
-                @pl.when(is_home)
+                @pl.when(carries)
                 def _():
                     for dx in range(1, chips):
                         x_copy(m, r, dx).wait_send()
 
-                for dg in range(1, n_grp):
-                    y_copy(m, r, dg).wait_send()
-                for h in range(n_grp):
-                    c_copy(m, r, h).wait_send()
+                for s in range(n_sub):
+                    for dg in range(1, n_grp):
+                        y_copy(m, r, dg, s).wait_send()
+                    for h in range(n_grp):
+                        c_copy(m, r, h, s).wait_send()
 
         pltpu.make_async_copy(served[m], outs[m], out_sem.at[m]).wait()
     for k in range(2):
@@ -363,16 +404,19 @@
     gate_shape, down_shape = (features, width), (d_rows, features)
     bf16 = functools.partial(jax.ShapeDtypeStruct, dtype=jnp.bfloat16)
     shapes = [(n_fs, owned, features)] + [gate_shape] * 4 + [down_shape] * 2
+    share = gate_first.shape[0] // n_grp
+    n_sub = chips if share % (16 * chips) == 0 else 1
     other_x, other_g = max(chips - 1, 1), max(n_grp - 1, 1)
     sems = [
-        (4, n_fs // n_tp), (4, n_fs), (4, n_fs, other_x), (4, n_fs), (4, n_fs, other_g),
-        (4, n_fs, n_grp), (4, n_fs, n_grp), (4, n_fs, n_grp), (4,),
+        (4, other_x), (4, other_x), (4, other_x, n_fs // n_tp),
+        (4, n_fs // n_tp), (4, n_fs), (4, n_fs, other_x), (4, n_fs, n_sub), (4, n_fs, other_g, n_sub),
+        (4, n_fs, n_grp, n_sub), (4, n_fs, n_grp, n_sub), (4, n_fs, n_grp, n_sub), (4,),
         (2, other_x), (2, other_x), (2, other_x, other_g), (2, other_x, other_g),
         (2, chips), (2, chips), (2,),
         (2, n_fs), (2, n_fs), (2, n_fs), (2, n_fs), (7,),
     ]
     result, g1, u1, g2, u2, d1, d2 = pl.pallas_call(
-        functools.partial(kernel, n_grp, n_fs, n_tp),
+        functools.partial(kernel, n_grp, n_fs, n_tp, n_sub),
         out_shape=[bf16(s) for s in shapes],
         in_specs=[pl.BlockSpec(memory_space=pltpu.VMEM)] + [pl.BlockSpec(memory_space=pl.ANY)] * 6,
         out_specs=[pl.BlockSpec(memory_space=pl.ANY)] * 7,
@@ -385,6 +429,7 @@
             pltpu.VMEM((2, n_fs, owned, features), jnp.bfloat16),
             pltpu.VMEM((2, n_fs, owned, features), jnp.bfloat16),
             pltpu.VMEM((2, n_fs, owned, features), jnp.bfloat16),
+            pltpu.VMEM((4, other_x, share // n_sub, gate_first.shape[1]), jnp.bfloat16),
         ]
         + [pltpu.SemaphoreType.DMA(s) for s in sems],
         compiler_params=pltpu.CompilerParams(

time: 270 us -> 254 us (0.941)
  the two profiles are of different devices: /device:TPU:0 before, /device:TPU:16 now
where the time goes in v2:
time: 254 us; the launch traced here: 253 us
  Pallas kernels  219 us (86%)
  local copies, waits for them, and re-layouts  24.8 us (10%)
  other arithmetic  8.68 us (3%)
    pallas_call x1, Pallas kernels, on_device(): pl.pallas_call(functools.partial(kernel, n_grp, n_fs, n_tp, n_sub), out_s...  219 us
    unnamed x23, local copies, waits for them, and re-layouts  24.8 us

profile of v2, /device:TPU:16, one launch (start us, length us, event | category | flops | bytes accessed | tf_op | source)
XLA Modules:
  0.0 253.2 jit_solution(10704216505199870883)
XLA Ops:
  0.6 0.0 copy-start.5
  0.6 0.0 copy-start.7
  0.7 2.8 %convert_element_type.22.refs_5_ = bf16[1024,512]{1,0:T(8,128)(2,1)} convert(f32[1024,512]{1,0:T(8,128)} %param.13) | non-fusion elementwise | flops 524288 | bytes 3145728 | tf_op jit(solution)/shard_map/convert_element_type | solution.py:396
  3.5 0.0 copy-done.5
  3.5 0.0 copy-start.6
  3.5 1.1 convert_element_type.23.refs_6_
  4.6 0.0 copy-done.7
  4.6 0.9 copy-done.6
  5.5 4.7 %multiply_convert_fusion = (bf16[512,1024]{1,0:T(8,128)(2,1)}, bf16[512,1024]{1,0:T(8,128)(2,1)}, bf16[512,1024]{1,0:T(8,128)(2,1)}, bf16[512,1024]{1,0:T(8,128)(2,1)}) fusion(f32[512,1024]{1,0:T(8,128)S(1)} %copy-done.6, f32[512]{0:T(512)} %param.14, f32[512,1024]{1,0:T(8,128)S(1)} %copy-done.7, f32[512,1024]{1,0:T(8,128)} %param.11, f32[512]{0:T(512)} %param.10, ...), kind=kLoop, calls=%fused_computation | loop fusion | flops 4194304 | bytes 12587008 | tf_op jit(solution)/shard_map/convert_element_type | solution.py:15
  10.2 219.1 %serve.1 = (bf16[4,64,2048]{2,1,0:T(8,128)(2,1)}, bf16[2048,1024]{1,0:T(8,128)(2,1)}, bf16[2048,1024]{1,0:T(8,128)(2,1)}, bf16[2048,1024]{1,0:T(8,128)(2,1)}, bf...) custom-call(bf16[256,2048]{1,0:T(8,128)(2,1)} %refs_0_.1, ...), custom_call_target="tpu_custom_call" | custom-call | tf_op jit(solution)/shard_map/serve/pallas_call | solution.py:418
  229.3 2.3 copy.23
  231.6 0.0 copy-start.4
  231.6 4.8 %copy.24 = bf16[2048,1024]{1,0:T(8,128)(2,1)} copy(bf16[2048,1024]{1,0:T(8,128)(2,1)} %get-tuple-element.35) | data formatting | bytes 8388608
  236.4 0.0 copy-done.4
  236.4 0.0 copy-start.3
  236.4 2.1 copy.25
  238.5 1.6 copy-done.3
  240.1 0.0 copy-start.2
  240.1 2.1 copy.26
  242.2 1.6 copy-done.2
  243.8 0.0 copy-start.1
  243.8 2.1 copy.27
  245.9 1.6 copy-done.1
  247.5 0.0 copy-start
  247.5 2.1 copy.28
  249.6 1.6 copy-done
  251.2 2.0 copy.29
Async XLA Ops:
  0.6 2.9 %copy-start.5 = (f32[1024,512]{1,0:T(8,128)S(1)}, f32[1024,512]{1,0:T(8,128)}, u32[]{:S(2)}) copy-start(f32[1024,512]{1,0:T(8,128)} %param.17) | copy-start | bytes 6291460
  0.6 4.0 %copy-start.7 = (f32[512,1024]{1,0:T(8,128)S(1)}, f32[512,1024]{1,0:T(8,128)}, u32[]{:S(2)}) copy-start(f32[512,1024]{1,0:T(8,128)} %param.15) | copy-start | bytes 6291460
  3.5 2.0 copy-start.6
  231.6 4.8 %copy-start.4 = (bf16[2048,1024]{1,0:T(8,128)(2,1)S(1)}, bf16[2048,1024]{1,0:T(8,128)(2,1)}, u32[]{:S(2)}) copy-start(bf16[2048,1024]{1,0:T(8,128)(2,1)} %get-tuple-element.36) | copy-start | bytes 12582916
  236.4 3.7 %copy-start.3 = (bf16[1024,2048]{1,0:T(8,128)(2,1)S(1)}, bf16[1024,2048]{1,0:T(8,128)(2,1)}, u32[]{:S(2)}) copy-start(bf16[1024,2048]{1,0:T(8,128)(2,1)} %get-tuple-element.37) | copy-start | bytes 12582916
  240.1 3.7 %copy-start.2 = (bf16[2048,1024]{1,0:T(8,128)(2,1)S(1)}, bf16[2048,1024]{1,0:T(8,128)(2,1)}, u32[]{:S(2)}) copy-start(bf16[2048,1024]{1,0:T(8,128)(2,1)} %get-tuple-element.38) | copy-start | bytes 12582916
  243.8 3.7 %copy-start.1 = (bf16[2048,1024]{1,0:T(8,128)(2,1)S(1)}, bf16[2048,1024]{1,0:T(8,128)(2,1)}, u32[]{:S(2)}) copy-start(bf16[2048,1024]{1,0:T(8,128)(2,1)} %get-tuple-element.39) | copy-start | bytes 12582916
  247.5 3.7 %copy-start = (bf16[1024,2048]{1,0:T(8,128)(2,1)S(1)}, bf16[1024,2048]{1,0:T(8,128)(2,1)}, u32[]{:S(2)}) copy-start(bf16[1024,2048]{1,0:T(8,128)(2,1)} %get-tuple-element.40) | copy-start | bytes 12582916
